TPU v7x, 32 devices: a whole 2x2x4 slice. The times are simulated.
32 devices in a mesh: sp: 4 (over z), tp: 2 (over y), dp: 4 (over x, core).
Axes of the slice: x: 2, y: 2, z: 4, core: 2. Of those that a mesh axis runs over, the one named last changes fastest.
Arguments:
- latent: bfloat16 [2048, 2048], P(('dp', 'sp', 'tp')), parts along dimension 0, may hold values from -6 to 6
- cond: bfloat16 [8192], P('dp'), parts along dimension 0, may hold values from -6 to 6
- context: bfloat16 [2048, 2048], P(('dp', 'sp')), parts along dimension 0, may hold values from -6 to 6
- context_cond: bfloat16 [2048], replicated, may hold values from -6 to 6
- modulation: bfloat16 [2048, 6144], P(('sp', 'tp')), may hold values from -0.125 to 0.125
- norm_gain: bfloat16 [2048], replicated, may hold values from 0.099609375 to 1.8984375
- w_x: bfloat16 [2048, 1024], P(None, 'tp'), may hold values from -0.125 to 0.125
- w_gate: bfloat16 [2048, 1024], P(None, 'tp'), may hold values from -0.125 to 0.125
- w_b: bfloat16 [2048, 256], P(None, 'tp'), may hold values from -0.125 to 0.125
- w_c: bfloat16 [2048, 256], P(None, 'tp'), may hold values from -0.125 to 0.125
- w_dt: bfloat16 [2, 2048, 16], P(None, None, 'tp'), may hold values from -0.125 to 0.125
- conv_x: bfloat16 [4, 1024], P(None, 'tp'), may hold values from -3 to 3
- conv_b: bfloat16 [4, 256], P(None, 'tp'), may hold values from -3 to 3
- conv_c: bfloat16 [4, 256], P(None, 'tp'), may hold values from -3 to 3
- decay_rate: float32 [2, 16], P(None, 'tp'), may hold values from 0 to 0.04
- decay_extra: float32 [2048, 16], P(('dp', 'sp'), 'tp'), parts along dimension 0, may hold values from -2 to 0
- out_gain: bfloat16 [1024], P('tp'), may hold values from 0.099609375 to 1.8984375
- w_out: bfloat16 [1024, 2048], replicated, may hold values from -0.1875 to 0.1875
Outputs:
- mixed: bfloat16 [2048, 2048], P(('dp', 'sp', 'tp')), parts along dimension 0
There are 4 independent parts, one for each index of `dp`. A program takes and returns all parts, laid end to end along the dimension named above; an argument that names none is the same for every part. Nothing has to cross between parts.
All inputs are finite; a program needn't handle non-finite values.
Results may differ from a plain program's by a relative error of at most 0.007.
Values may be sent and summed in bfloat16 or wider, within the bound.
A program may use at most 64 MiB of HBM per device.

v0:
```python
import jax
import jax.numpy as jnp
from jax import lax
from jax.sharding import PartitionSpec as P

HEAD_DIM = 64
STATE = 64
BLOCK = 128
ROW_EPS = 1e-06
GROUP_EPS = 1e-05
HIGHEST = lax.Precision.HIGHEST


def prefix(x, axis, join, neutral, backward):
    count = lax.axis_size(axis)
    place = lax.axis_index(axis)
    ahead = count - 1 - place if backward else place
    gathered = jax.tree.map(
        lambda a, kind: lax.all_gather(a.astype(kind), axis),
        x,
        jax.tree.map(lambda a: jnp.bfloat16 if a.dtype == jnp.float32 else a.dtype, x),
    )
    state = jax.tree.map(lambda a, e: jnp.zeros_like(a) + jnp.asarray(e, a.dtype), x, neutral)

    def one(hop, state):
        source = count - 1 - hop if backward else hop
        return join(
            state,
            jax.tree.map(
                lambda a, own: lax.dynamic_index_in_dim(a, source, 0, False).astype(own.dtype),
                gathered,
                x,
            ),
        )

    return lax.fori_loop(0, ahead, one, state)


def with_halo(block, sides, width):
    for axis, dim in sides:
        count = lax.axis_size(axis)
        forward = [(i, i + 1) for i in range(count - 1)]
        backward = [(target, source) for source, target in forward]
        low = lax.ppermute(
            lax.slice_in_dim(block, block.shape[dim] - width, None, axis=dim), axis, forward
        )
        high = lax.ppermute(lax.slice_in_dim(block, 0, width, axis=dim), axis, backward)
        block = jnp.concatenate([low, block, high], axis=dim)
    return block


def modulated_norm(row_block, norm_gain, shift_row, scale_row):
    values = row_block.astype(jnp.float32)
    normed = values * lax.rsqrt(jnp.mean(values * values, axis=-1, keepdims=True) + ROW_EPS)
    return (normed * norm_gain.astype(jnp.float32) * (1.0 + scale_row) + shift_row).astype(
        jnp.bfloat16
    )


def project_many(row_block, weights):
    return jnp.concatenate(
        [
            jnp.dot(row_block, weight, preferred_element_type=jnp.float32).astype(jnp.bfloat16)
            for weight in weights
        ],
        axis=1,
    )


def conv_padded(padded, conv_taps, length):
    values = padded.astype(jnp.float32)
    summed = jnp.zeros((length, values.shape[1]), jnp.float32)
    for offset in range(conv_taps.shape[0]):
        summed = summed + conv_taps[offset].astype(jnp.float32) * values[offset : offset + length]
    return jax.nn.silu(summed).astype(jnp.bfloat16)


def context_states(ctx_xs, ctx_bmat, ctx_dt, decay_rate):
    length = ctx_xs.shape[0]
    groups = ctx_bmat.shape[1] // STATE
    heads_here = ctx_dt.shape[2]
    repeat = heads_here // groups
    values = ctx_xs.astype(jnp.float32).reshape(length, groups, repeat, HEAD_DIM)
    keys_b = ctx_bmat.astype(jnp.float32).reshape(length, groups, STATE)
    log_decay = -decay_rate[:, None, :] * ctx_dt
    running = jnp.cumsum(log_decay, axis=1)
    forward_weight = (jnp.exp(running[0, -1:] - running[0]) * ctx_dt[0]).reshape(
        length, groups, repeat
    )
    backward_weight = (jnp.exp(running[1] - log_decay[1]) * ctx_dt[1]).reshape(
        length, groups, repeat
    )
    forward_state = jnp.einsum(
        "lgn,lgr,lgrp->grpn", keys_b, forward_weight, values, precision=HIGHEST
    )
    backward_state = jnp.einsum(
        "lgn,lgr,lgrp->grpn", keys_b, backward_weight, values, precision=HIGHEST
    )
    return (forward_state, backward_state)


def block_pass(inputs, step_sizes, log_decay, bmat, cmat, start_state):
    length = inputs.shape[0]
    groups, repeat = (start_state.shape[0], start_state.shape[1])
    block_count = length // BLOCK
    values = inputs.reshape(block_count, BLOCK, groups, repeat, HEAD_DIM)
    steps_blk = step_sizes.reshape(block_count, BLOCK, groups, repeat)
    decays = log_decay.reshape(block_count, BLOCK, groups, repeat)
    keys_b = bmat.reshape(block_count, BLOCK, groups, STATE)
    reads_c = cmat.reshape(block_count, BLOCK, groups, STATE)
    lower_mask = (jnp.arange(BLOCK)[:, None] >= jnp.arange(BLOCK)[None, :])[:, :, None, None]

    def advance(carried, block_data):
        value_blk, step_blk, decay_blk, key_blk, read_blk = block_data
        running = jnp.cumsum(decay_blk, axis=0)
        log_gaps = running[:, None] - running[None, :]
        mixing = jnp.where(lower_mask, jnp.exp(jnp.where(lower_mask, log_gaps, 0.0)), 0.0)
        affinity = jnp.einsum("ign,jgn->ijg", read_blk, key_blk, preferred_element_type=jnp.float32)
        weights = (affinity[..., None] * mixing * step_blk[None]).astype(jnp.bfloat16)
        output = jnp.einsum(
            "ijgr,jgrp->igrp", weights, value_blk, preferred_element_type=jnp.float32
        )
        output = output + jnp.einsum(
            "ign,grpn,igr->igrp",
            read_blk.astype(jnp.float32),
            carried,
            jnp.exp(running),
            precision=HIGHEST,
        )
        to_end = jnp.exp(running[-1:] - running) * step_blk
        state_in = (key_blk.astype(jnp.float32)[:, :, None, :] * to_end[..., None]).astype(
            jnp.bfloat16
        )
        carried = jnp.exp(running[-1])[..., None, None] * carried + jnp.einsum(
            "jgrn,jgrp->grpn", state_in, value_blk, preferred_element_type=jnp.float32
        )
        return (carried, output)

    final_state, outputs = lax.scan(
        advance, start_state, (values, steps_blk, decays, keys_b, reads_c)
    )
    return (outputs.reshape(length, groups, repeat, HEAD_DIM), final_state)


def state_chain(summary, backward):

    def combine(earlier, later_part):
        return (
            earlier[0] + later_part[0],
            jnp.exp(later_part[0])[..., None, None] * earlier[1] + later_part[1],
        )

    identity_pair = (jnp.zeros_like(summary[0]), jnp.zeros_like(summary[1]))
    return prefix(summary, "sp", combine, identity_pair, backward)


def directed_pass(inputs, step_sizes, log_decay, bmat, cmat, outer_start, zeros_state, backward):
    local_out, final_state = block_pass(inputs, step_sizes, log_decay, bmat, cmat, zeros_state)
    length = inputs.shape[0]
    groups, repeat = (zeros_state.shape[0], zeros_state.shape[1])
    running = jnp.cumsum(log_decay, axis=0).reshape(length, groups, repeat)
    before = state_chain((running[-1], final_state), backward)
    entry_state = jnp.exp(before[0])[..., None, None] * outer_start + before[1]
    read_rows = cmat.astype(jnp.float32).reshape(length, groups, STATE)
    return local_out + jnp.einsum(
        "tgn,grpn,tgr->tgrp", read_rows, entry_state, jnp.exp(running), precision=HIGHEST
    )


def group_norm(combined, out_gain):
    length, groups, repeat, _ = combined.shape
    mean_square = jnp.mean(combined * combined, axis=(2, 3), keepdims=True)
    scaled = (
        combined
        * lax.rsqrt(mean_square + GROUP_EPS)
        * out_gain.astype(jnp.float32).reshape(groups, repeat, HEAD_DIM)
    )
    return scaled.reshape(length, groups * repeat * HEAD_DIM).astype(jnp.bfloat16)


def local(
    latent,
    cond,
    context,
    context_cond,
    modulation,
    norm_gain,
    w_x,
    w_gate,
    w_b,
    w_c,
    w_dt,
    conv_x,
    conv_b,
    conv_c,
    decay_rate,
    decay_extra,
    out_gain,
    w_out,
):
    model_width = latent.shape[1]
    mod_share = modulation.shape[0]
    cond_rows = jax.nn.silu(jnp.stack([cond, context_cond]).astype(jnp.float32)).astype(
        jnp.bfloat16
    )
    own_cols = lax.dynamic_slice_in_dim(
        cond_rows, lax.axis_index(("sp", "tp")) * mod_share, mod_share, 1
    )
    mod_rows = lax.psum(
        jnp.dot(own_cols, modulation, preferred_element_type=jnp.float32), ("sp", "tp")
    )
    shift_rows = mod_rows[:, :model_width]
    scale_rows = mod_rows[:, model_width : 2 * model_width]
    gate_row = mod_rows[0, 2 * model_width :]
    head_cols = w_x.shape[1]
    state_cols = w_b.shape[1]
    heads_here = w_dt.shape[2]
    groups_here = state_cols // STATE
    repeat = heads_here // groups_here
    hidden = modulated_norm(latent, norm_gain, shift_rows[0], scale_rows[0])
    latent_mats = (w_x, w_b, w_c, w_gate, w_dt[0], w_dt[1])
    projected = project_many(lax.all_gather(hidden, "tp", axis=0, tiled=True), latent_mats)
    token_count = projected.shape[0]
    conv_cols = head_cols + 2 * state_cols
    extended = with_halo(projected[:, :conv_cols], (("sp", 0),), 2)
    conv_taps = jnp.concatenate([conv_x, conv_b, conv_c], axis=1)
    convolved = conv_padded(extended, conv_taps, token_count)
    latent_xs = convolved[:, :head_cols]
    latent_b = convolved[:, head_cols : head_cols + state_cols]
    latent_c = convolved[:, head_cols + state_cols :]
    gate_in = projected[:, conv_cols : conv_cols + head_cols]
    dt_start = conv_cols + head_cols
    latent_dt = jnp.stack(
        [
            jax.nn.softplus(projected[:, dt_start : dt_start + heads_here].astype(jnp.float32)),
            jax.nn.softplus(projected[:, dt_start + heads_here :].astype(jnp.float32)),
        ]
    )
    context_mats = (w_x, w_b, w_dt[0], w_dt[1])
    own_context = project_many(
        modulated_norm(context, norm_gain, shift_rows[1], scale_rows[1]), context_mats
    )
    context_cols = lax.all_gather(own_context, "sp", axis=0, tiled=True)
    ctx_span = head_cols + state_cols
    ctx_padded = jnp.pad(context_cols[:, :ctx_span], ((2, 1), (0, 0)))
    ctx_conv = conv_padded(
        ctx_padded, jnp.concatenate([conv_x, conv_b], axis=1), context_cols.shape[0]
    )
    ctx_dt = jnp.stack(
        [
            jax.nn.softplus(context_cols[:, ctx_span : ctx_span + heads_here].astype(jnp.float32)),
            jax.nn.softplus(context_cols[:, ctx_span + heads_here :].astype(jnp.float32)),
        ]
    )
    forward_start, backward_start = context_states(
        ctx_conv[:, :head_cols], ctx_conv[:, head_cols:], ctx_dt, decay_rate
    )
    log_decay = -decay_rate[:, None, :] * latent_dt + decay_extra[None]
    zeros_state = jnp.zeros((groups_here, repeat, HEAD_DIM, STATE), jnp.float32)
    y_forward = directed_pass(
        latent_xs, latent_dt[0], log_decay[0], latent_b, latent_c, forward_start, zeros_state, False
    )
    y_backward = directed_pass(
        latent_xs[::-1],
        latent_dt[1][::-1],
        log_decay[1][::-1],
        latent_b[::-1],
        latent_c[::-1],
        backward_start,
        zeros_state,
        True,
    )
    gate_act = jax.nn.silu(gate_in.astype(jnp.float32)).reshape(
        token_count, groups_here, repeat, HEAD_DIM
    )
    combined = (y_forward + y_backward[::-1]) * gate_act
    normed = group_norm(combined, out_gain)
    tp_count = lax.axis_size("tp")
    stacked = normed.reshape(tp_count, token_count // tp_count, normed.shape[1])
    branch = jnp.dot(
        lax.all_to_all(stacked, "tp", split_axis=0, concat_axis=2, tiled=True)[0],
        w_out,
        preferred_element_type=jnp.float32,
    )[None]
    return (latent.astype(jnp.float32) + gate_row * branch[0]).astype(jnp.bfloat16)


def solution(mesh):
    in_specs = (
        P(("dp", "sp", "tp"), None),
        P("dp"),
        P(("dp", "sp"), None),
        P(),
        P(("sp", "tp"), None),
        P(),
        P(None, "tp"),
        P(None, "tp"),
        P(None, "tp"),
        P(None, "tp"),
        P(None, None, "tp"),
        P(None, "tp"),
        P(None, "tp"),
        P(None, "tp"),
        P(None, "tp"),
        P(("dp", "sp"), "tp"),
        P("tp"),
        P(),
    )
    out_specs = P(("dp", "sp", "tp"), None)
    return jax.shard_map(local, mesh=mesh, in_specs=in_specs, out_specs=out_specs, check_vma=False)
```

profile of v0, /device:TPU:0, one launch (start us, length us, event | category | flops | bytes accessed | tf_op | source)
XLA Modules:
  0.0 247.8 jit_solution(15845269503590403432)
XLA Ops:
  2.4 39.4 %psum.7 = f32[2,6144]{1,0:T(2,128)S(1)} all-reduce(f32[2,6144]{1,0:T(2,128)S(1)} %fusion.93), channel_id=1, replica_groups=mesh['sp'=4,'tp'=2,'dp'=4] {'sp','tp'}, use_global_device_ids=true, to_apply=%region_0.1 | all-reduce | flops 12288 | bytes 98304 | tf_op jit(solution)/shard_map/psum | solution.py:209
  42.9 7.2 %all_gather.26 = bf16[128,2048]{1,0:T(8,128)(2,1)S(1)} all-gather(bf16[64,2048]{1,0:T(8,128)(2,1)S(1)} %fusion.31), channel_id=1, replica_groups=mesh['sp'=4,'tp'=2,'dp'=4] {'tp'}, dimensions={0}, use_global_device_ids=true | all-gather | bytes 786432 | tf_op jit(solution)/shard_map/all_gather | solution.py:222
  50.0 2.3 convolution_convert_fusion.2
  53.6 1.9 collective-permute-start
  55.4 1.3 collective-permute-start.1
  60.7 2.9 %convolution_convert_fusion.1 = bf16[128,512]{0,1:T(8,128)(2,1)S(1)} fusion(bf16[2048,512]{1,0:T(8,128)(2,1)} %param.28, bf16[128,2048]{1,0:T(8,128)(2,1)} %param.24, f32[2048]{0:T(1024)} %bitcast.249, f32[2048]{0:T(1024)} %bitcast.253, f32[2048]{0:T(1024)S(1)} %convert_element_type.221, f32[128]{0:T(128)S(1)} %add_rsqrt_fusion.1), kind=kOutput, calls=%fused_computation.49 | convolution fusion | flops 270073856 | bytes 2777600 | tf_op jit(solution)/shard_map/dot_general | solution.py:63
  65.2 14.5 %all_gather.30 = bf16[512,656]{0,1:T(8,128)(2,1)S(1)} all-gather(bf16[128,656]{0,1:T(8,128)(2,1)S(1)} %pad_maximum_fusion), channel_id=1, replica_groups=mesh['sp'=4,'tp'=2,'dp'=4] {'sp'}, dimensions={0}, use_global_device_ids=true | all-gather | bytes 839680 | tf_op jit(solution)/shard_map/all_gather | solution.py:243
  90.8 1.6 reduce_window_sum.52
  93.7 5.0 %reduce-window.6 = f32[2,8,4,128]{3,1,2,0:T(8,128)} reduce-window(f32[2,8,4,128]{3,1,2,0:T(8,128)} %fusion.148, f32[]{:T(128)} %constant.128.clone.1), window={size=1x1x1x128 pad=0_0x0_0x0_0x127_0}, to_apply=%region_7.8 | reduce-window | flops 1040384 | bytes 65540 | tf_op jit(solution)/shard_map/reduce-window
  98.7 1.5 slice_reduce_fusion
  103.1 2.7 %pad_convert_fusion = f32[515,640]{0,1:T(8,128)} fusion(bf16[512,640]{0,1:T(8,128)(2,1)} %slice.222), kind=kLoop, calls=%fused_computation.67 | loop fusion | flops 329600 | bytes 1973760 | tf_op jit(solution)/shard_map/convert_element_type | solution.py:71
  107.2 1.6 reduce_window_sum.56
  110.2 3.1 %divide_multiply_fusion = f32[128,512]{1,0:T(8,128)} fusion(bf16[128,2048]{1,0:T(8,128)(2,1)} %copy-done.2, bf16[2048,512]{1,0:T(8,128)(2,1)} %param.29), kind=kOutput, calls=%fused_computation.89 | convolution fusion | flops 268828672 | bytes 2883584 | tf_op jit(solution)/shard_map/dot_general | solution.py:63
  113.3 1.4 fusion.76
  116.3 2.4 multiply_convert_fusion
  118.7 10.4 %all_gather.27 = bf16[4,2,4]{2,1,0:T(2,128)(2,1)} all-gather(bf16[1,2,4]{2,1,0:T(2,128)(2,1)S(1)} %copy-done.55), channel_id=1, replica_groups=mesh['sp'=4,'tp'=2,'dp'=4] {'sp'}, dimensions={0}, use_global_device_ids=true | all-gather | bytes 80 | tf_op jit(solution)/shard_map/all_gather | solution.py:19
  129.1 8.0 %all_gather.31 = bf16[4,2,4]{2,1,0:T(2,128)(2,1)} all-gather(bf16[1,2,4]{2,1,0:T(2,128)(2,1)S(1)} %copy-done.56), channel_id=1, replica_groups=mesh['sp'=4,'tp'=2,'dp'=4] {'sp'}, dimensions={0}, use_global_device_ids=true | all-gather | bytes 80 | tf_op jit(solution)/shard_map/all_gather | solution.py:19
  137.1 1.9 slice.230
  139.0 1.6 slice.231
  140.5 1.5 exp.128
  142.0 1.5 exp.139
  145.8 1.4 reshape.201
  147.2 1.5 copy.174
  148.7 1.3 reshape.203
  150.0 1.6 copy.189
  151.6 1.5 copy.187
  153.1 1.6 copy.185
  154.6 1.6 copy.172
  156.2 1.8 copy.190
  158.0 1.3 reshape.218
  160.6 1.3 rev.18
  164.3 16.6 %all-gather = bf16[8,4,64,64]{3,2,1,0:T(8,128)(2,1)} all-gather(bf16[2,4,64,64]{3,2,1,0:T(8,128)(2,1)S(1)} %fusion.17), channel_id=2, replica_groups=mesh['sp'=4,'tp'=2,'dp'=4] {'sp'}, dimensions={0}, use_global_device_ids=true | all-gather | bytes 327680 | tf_op jit(solution)/shard_map/all_gather | solution.py:19
  182.7 1.6 copy.178
  184.3 1.5 copy.179
  187.7 19.2 %all-gather.1 = bf16[8,4,64,64]{3,2,1,0:T(8,128)(2,1)} all-gather(bf16[2,4,64,64]{3,2,1,0:T(8,128)(2,1)S(1)} %fusion.18), channel_id=3, replica_groups=mesh['sp'=4,'tp'=2,'dp'=4] {'sp'}, dimensions={0}, use_global_device_ids=true | all-gather | bytes 327680 | tf_op jit(solution)/shard_map/all_gather | solution.py:19
  207.5 7.0 %while.7 = (s32[]{:T(128)}, f32[2,4]{1,0:T(2,128)}, f32[2,4,64,64]{3,2,1,0:T(8,128)S(1)}, s32[]{:T(128)}, bf16[4,2,4]{2,1,0:T(2,128)(2,1)}, /*index=5*/bf16[4,2,...) while((s32[]{:T(128)}, f32[2,4]{1,0:T(2,128)}, f32[2,4,64,64]{3,2,1,0:T(8,128)S(1)}, ...), condition=%wide.region_12.13_spmd, body=%wide.region_11.12_spmd.sunk | while | flops 98326 | bytes 327979 | solution.py:36
  209.7 1.3 convert_exponential_fusion.5
  214.5 1.3 exp.143
  215.8 1.5 copy.180
  217.2 1.6 convolution_bitcast_fusion.6
  218.9 1.6 copy.181
  221.6 1.7 fusion.15
  225.5 1.8 rev.23
  227.3 1.6 convolution_bitcast_fusion.7
  229.0 1.7 copy.168
  231.7 1.7 fusion.16
  237.0 6.8 %all_to_all.15 = bf16[2,64,512]{2,1,0:T(8,128)(2,1)S(1)} all-to-all(bf16[2,64,512]{2,1,0:T(8,128)(2,1)S(1)} %copy.199), channel_id=1, replica_groups=mesh['sp'=4,'tp'=2,'dp'=4] {'tp'}, dimensions={0} | all-to-all | bytes 262144 | tf_op jit(solution)/shard_map/all_to_all | solution.py:281
  244.1 3.8 %fusion.1 = bf16[64,2048]{1,0:T(8,128)(2,1)} fusion(bf16[64,1024]{1,0:T(8,128)(2,1)S(1)} %bitcast.213, bf16[1024,2048]{1,0:T(8,128)(2,1)} %param.39, bf16[64,2048]{1,0:T(8,128)(2,1)S(1)} %copy-done.7, f32[2048]{0:T(1024)S(1)} %bitcast.239), kind=kOutput, calls=%fused_computation.10 | convolution fusion | flops 268959744 | bytes 4857856 | tf_op jit(solution)/shard_map/dot_general | solution.py:280
  (214 shorter events, 53.2 us)
Async XLA Ops:
  1.9 40.6 %copy-start.48 = (bf16[2048]{0:T(1024)(128)(2,1)S(1)}, bf16[2048]{0:T(1024)(128)(2,1)}, u32[]{:S(2)}) copy-start(bf16[2048]{0:T(1024)(128)(2,1)} %param.27) | copy-start | bytes 12292
  1.9 40.6 %copy-start.6 = (bf16[64,2048]{1,0:T(8,128)(2,1)S(1)}, bf16[64,2048]{1,0:T(8,128)(2,1)}, u32[]{:S(2)}) copy-start(bf16[64,2048]{1,0:T(8,128)(2,1)} %param.22) | copy-start | bytes 786436
  42.8 9.4 %copy-start.11 = (bf16[2048,128]{1,0:T(8,128)(2,1)S(1)}, bf16[2048,128]{1,0:T(8,128)(2,1)}, u32[]{:S(2)}) copy-start(bf16[2048,128]{1,0:T(8,128)(2,1)} %param.31) | copy-start | bytes 1572868
  50.0 7.0 %copy-start.2 = (bf16[128,2048]{1,0:T(8,128)(2,1)}, bf16[128,2048]{1,0:T(8,128)(2,1)S(1)}, u32[]{:S(2)}) copy-start(bf16[128,2048]{1,0:T(8,128)(2,1)S(1)} %all_gather.26) | copy-start | bytes 1572868
  52.3 4.4 %copy-start.27 = (bf16[2,2048,8]{1,2,0:T(8,128)(2,1)S(1)}, bf16[2,2048,8]{1,2,0:T(8,128)(2,1)}, u32[]{:S(2)}) copy-start(bf16[2,2048,8]{1,2,0:T(8,128)(2,1)} %param.32) | copy-start | bytes 196612
  52.3 4.9 %copy-start.54 = (f32[2,8]{1,0:T(2,128)S(1)}, f32[2,8]{1,0:T(2,128)}, u32[]{:S(2)}) copy-start(f32[2,8]{1,0:T(2,128)} %param.36) | copy-start | bytes 196
  52.3 5.0 %copy-start.52 = (f32[128,8]{0,1:T(8,128)S(1)}, f32[128,8]{0,1:T(8,128)}, u32[]{:S(2)}) copy-start(f32[128,8]{0,1:T(8,128)} %param.37) | copy-start | bytes 12292
  52.6 5.3 %copy-start.18 = (bf16[128,128]{1,0:T(8,128)(2,1)}, bf16[128,128]{1,0:T(8,128)(2,1)S(1)}, u32[]{:S(2)}) copy-start(bf16[128,128]{1,0:T(8,128)(2,1)S(1)} %convolution_convert_fusion.4) | copy-start | bytes 98308
  52.9 5.0 %copy-start.19 = (bf16[128,128]{1,0:T(8,128)(2,1)}, bf16[128,128]{1,0:T(8,128)(2,1)S(1)}, u32[]{:S(2)}) copy-start(bf16[128,128]{1,0:T(8,128)(2,1)S(1)} %convolution_convert_fusion.5) | copy-start | bytes 98308
  53.6 105.8 %collective-permute-start = (bf16[2,768]{1,0:T(2,128)(2,1)}, bf16[2,768]{1,0:T(2,128)(2,1)}, u32[]{:S(2)}, u32[]{:S(2)}) collective-permute-start(bf16[2,768]{1,0:T(2,128)(2,1)} %get-tuple-element.220), channel_id=1, source_target_pairs={{0,8},{8,16},{16,24},{1,9},{9,17},{17,25},{2,10},{10,18},{18,26},{... | collective-permute-start | bytes 9224 | tf_op jit(solution)/shard_map/ppermute | solution.py:44
  55.4 103.9 %collective-permute-start.1 = (bf16[2,768]{1,0:T(2,128)(2,1)}, bf16[2,768]{1,0:T(2,128)(2,1)}, u32[]{:S(2)}, u32[]{:S(2)}) collective-permute-start(bf16[2,768]{1,0:T(2,128)(2,1)} %get-tuple-element.221), channel_id=1, source_target_pairs={{8,0},{16,8},{24,16},{9,1},{17,9},{25,17},{10,2},{18,10},{26,18},{... | collective-permute-start | bytes 9224 | tf_op jit(solution)/shard_map/ppermute | solution.py:47
  57.0 29.6 %copy-start.25 = (f32[128,8]{0,1:T(8,128)}, f32[128,8]{0,1:T(8,128)S(1)}, u32[]{:S(2)}) copy-start(f32[128,8]{0,1:T(8,128)S(1)} %compare_select_fusion.3) | copy-start | bytes 12292
  64.8 14.9 %copy-start.37 = (f32[2,8]{1,0:T(2,128)S(1)}, f32[2,8]{1,0:T(2,128)}, u32[]{:S(2)}) copy-start(f32[2,8]{1,0:T(2,128)} %copy-done.36) | copy-start | bytes 196
  65.2 17.6 %copy-start.41 = (f32[128,8]{0,1:T(8,128)S(1)}, f32[128,8]{0,1:T(8,128)}, u32[]{:S(2)}) copy-start(f32[128,8]{0,1:T(8,128)} %get-tuple-element.233) | copy-start | bytes 12292
  65.2 24.9 %copy-start.38 = (f32[128,8]{0,1:T(8,128)S(1)}, f32[128,8]{0,1:T(8,128)}, u32[]{:S(2)}) copy-start(f32[128,8]{0,1:T(8,128)} %get-tuple-element.232) | copy-start | bytes 12292
  100.9 5.5 %copy-start.39 = (f32[128,8]{0,1:T(8,128)S(1)}, f32[128,8]{0,1:T(8,128)}, u32[]{:S(2)}) copy-start(f32[128,8]{0,1:T(8,128)} %rev.22) | copy-start | bytes 12292
  110.2 3.2 %copy-start.22 = (f32[2,512,8]{1,2,0:T(8,128)S(1)}, f32[2,512,8]{1,2,0:T(8,128)}, u32[]{:S(2)}) copy-start(f32[2,512,8]{1,2,0:T(8,128)} %copy-done.21) | copy-start | bytes 98308
  110.2 3.2 %copy-start.24 = (f32[2,512,8]{1,2,0:T(8,128)S(1)}, f32[2,512,8]{1,2,0:T(8,128)}, u32[]{:S(2)}) copy-start(f32[2,512,8]{1,2,0:T(8,128)} %maximum_multiply_fusion) | copy-start | bytes 98308
  110.2 3.2 %copy-start.53 = (f32[8]{0:T(128)S(1)}, f32[8]{0:T(128)}, u32[]{:S(2)}) copy-start(f32[8]{0:T(128)} %slice_reduce_fusion.1) | copy-start | bytes 100
  110.2 4.6 %copy-start.50 = (f32[2,4]{1,0:T(2,128)S(1)}, f32[2,4]{1,0:T(2,128)}, u32[]{:S(2)}) copy-start(f32[2,4]{1,0:T(2,128)} %slice_bitcast_fusion.3) | copy-start | bytes 100
  110.2 4.6 %copy-start.15 = (f32[128,2,4]{2,1,0:T(2,128)S(1)}, f32[128,2,4]{2,1,0:T(2,128)}, u32[]{:S(2)}) copy-start(f32[128,2,4]{2,1,0:T(2,128)} %copy.175) | copy-start | bytes 12292
  110.2 5.3 %copy-start.51 = (f32[2,4]{1,0:T(2,128)S(1)}, f32[2,4]{1,0:T(2,128)}, u32[]{:S(2)}) copy-start(f32[2,4]{1,0:T(2,128)} %slice_bitcast_fusion.2) | copy-start | bytes 100
  110.2 5.3 %copy-start.16 = (f32[128,2,4]{2,1,0:T(2,128)S(1)}, f32[128,2,4]{2,1,0:T(2,128)}, u32[]{:S(2)}) copy-start(f32[128,2,4]{2,1,0:T(2,128)} %copy.188) | copy-start | bytes 12292
  110.2 6.1 %copy-start.1 = (f32[515,640]{0,1:T(8,128)S(1)}, f32[515,640]{0,1:T(8,128)}, u32[]{:S(2)}) copy-start(f32[515,640]{0,1:T(8,128)} %pad_convert_fusion) | copy-start | bytes 3955204
  110.2 6.1 %copy-start.42 = (f32[640]{0:T(1024)S(1)}, f32[640]{0:T(1024)}, u32[]{:S(2)}) copy-start(f32[640]{0:T(1024)} %get-tuple-element.183) | copy-start | bytes 7684
  110.2 6.1 %copy-start.43 = (f32[640]{0:T(1024)S(1)}, f32[640]{0:T(1024)}, u32[]{:S(2)}) copy-start(f32[640]{0:T(1024)} %get-tuple-element.184) | copy-start | bytes 7684
  110.2 6.1 %copy-start.44 = (f32[640]{0:T(1024)S(1)}, f32[640]{0:T(1024)}, u32[]{:S(2)}) copy-start(f32[640]{0:T(1024)} %get-tuple-element.185) | copy-start | bytes 7684
  116.3 12.8 %copy-start.56 = (bf16[1,2,4]{2,1,0:T(2,128)(2,1)S(1)}, bf16[1,2,4]{2,1,0:T(2,128)(2,1)}, u32[]{:S(2)}) copy-start(bf16[1,2,4]{2,1,0:T(2,128)(2,1)} %convert_element_type.248) | copy-start | bytes 52
  144.2 16.0 %copy-start.31 = (f32[768]{0:T(1024)S(1)}, f32[768]{0:T(1024)}, u32[]{:S(2)}) copy-start(f32[768]{0:T(1024)} %get-tuple-element.178) | copy-start | bytes 9220
  144.2 16.0 %copy-start.32 = (f32[768]{0:T(1024)S(1)}, f32[768]{0:T(1024)}, u32[]{:S(2)}) copy-start(f32[768]{0:T(1024)} %get-tuple-element.179) | copy-start | bytes 9220
  144.2 16.0 %copy-start.33 = (f32[768]{0:T(1024)S(1)}, f32[768]{0:T(1024)}, u32[]{:S(2)}) copy-start(f32[768]{0:T(1024)} %get-tuple-element.180) | copy-start | bytes 9220
  144.2 16.0 %copy-start.34 = (f32[768]{0:T(1024)S(1)}, f32[768]{0:T(1024)}, u32[]{:S(2)}) copy-start(f32[768]{0:T(1024)} %get-tuple-element.181) | copy-start | bytes 9220
  160.2 3.9 %copy-start.47 = (f32[2,4]{1,0:T(2,128)S(1)}, f32[2,4]{1,0:T(2,128)}, u32[]{:S(2)}) copy-start(f32[2,4]{1,0:T(2,128)} %exponential_multiply_fusion.3) | copy-start | bytes 100
  162.1 18.8 %copy-start.20 = (bf16[128,128]{0,1:T(8,128)(2,1)}, bf16[128,128]{0,1:T(8,128)(2,1)S(1)}, u32[]{:S(2)}) copy-start(bf16[128,128]{0,1:T(8,128)(2,1)S(1)} %copy.166) | copy-start | bytes 98308
  181.5 25.4 %copy-start.3 = (f32[2,4,64,64]{3,2,1,0:T(8,128)}, f32[2,4,64,64]{3,2,1,0:T(8,128)S(1)}, u32[]{:S(2)}) copy-start(f32[2,4,64,64]{3,2,1,0:T(8,128)S(1)} %get-tuple-element.175) | copy-start | bytes 393220
  220.5 3.9 %copy-start.14 = (bf16[128,512]{0,1:T(8,128)(2,1)S(1)}, bf16[128,512]{0,1:T(8,128)(2,1)}, u32[]{:S(2)}) copy-start(bf16[128,512]{0,1:T(8,128)(2,1)} %copy.178) | copy-start | bytes 393220
  220.5 3.9 %copy-start.23 = (f32[128,128,2]{1,0,2:T(8,128)S(1)}, f32[128,128,2]{1,0,2:T(8,128)}, u32[]{:S(2)}) copy-start(f32[128,128,2]{1,0,2:T(8,128)} %copy.181) | copy-start | bytes 393220
  220.5 3.9 %copy-start.40 = (f32[128,8]{0,1:T(8,128)S(1)}, f32[128,8]{0,1:T(8,128)}, u32[]{:S(2)}) copy-start(f32[128,8]{0,1:T(8,128)} %rev.22) | copy-start | bytes 12292
  220.5 3.9 %copy-start.49 = (f32[128,2,4]{0,2,1:T(4,128)S(1)}, f32[128,2,4]{0,2,1:T(4,128)}, u32[]{:S(2)}) copy-start(f32[128,2,4]{0,2,1:T(4,128)} %copy.183) | copy-start | bytes 12292
  223.3 8.4 %copy-start.4 = (f32[2,4,64,64]{3,2,1,0:T(8,128)S(1)}, f32[2,4,64,64]{3,2,1,0:T(8,128)}, u32[]{:S(2)}) copy-start(f32[2,4,64,64]{3,2,1,0:T(8,128)} %copy-done.3) | copy-start | bytes 393220
  230.6 3.9 %copy-start.8 = (f32[128,512]{0,1:T(8,128)S(1)}, f32[128,512]{0,1:T(8,128)}, u32[]{:S(2)}) copy-start(f32[128,512]{0,1:T(8,128)} %copy.190) | copy-start | bytes 786436
  230.6 3.9 %copy-start.9 = (f32[128,2,4,64]{0,3,2,1:T(8,128)S(1)}, f32[128,2,4,64]{0,3,2,1:T(8,128)}, u32[]{:S(2)}) copy-start(f32[128,2,4,64]{0,3,2,1:T(8,128)} %rev.23) | copy-start | bytes 786436
  230.6 3.9 %copy-start.17 = (f32[128,128,2]{1,0,2:T(8,128)S(1)}, f32[128,128,2]{1,0,2:T(8,128)}, u32[]{:S(2)}) copy-start(f32[128,128,2]{1,0,2:T(8,128)} %copy.168) | copy-start | bytes 393220
  230.6 3.9 %copy-start.26 = (f32[128,8]{0,1:T(8,128)S(1)}, f32[128,8]{0,1:T(8,128)}, u32[]{:S(2)}) copy-start(f32[128,8]{0,1:T(8,128)} %copy-done.25) | copy-start | bytes 12292
  230.6 3.9 %copy-start.29 = (f32[128,2,4]{0,2,1:T(4,128)S(1)}, f32[128,2,4]{0,2,1:T(4,128)}, u32[]{:S(2)}) copy-start(f32[128,2,4]{0,2,1:T(4,128)} %copy.170) | copy-start | bytes 12292
  231.7 3.2 %copy-start.35 = (f32[2,4,64]{2,1,0:T(4,128)S(1)}, f32[2,4,64]{2,1,0:T(4,128)}, u32[]{:S(2)}) copy-start(f32[2,4,64]{2,1,0:T(4,128)} %reshape.218) | copy-start | bytes 6148
  234.5 9.5 %copy-start.7 = (bf16[64,2048]{1,0:T(8,128)(2,1)S(1)}, bf16[64,2048]{1,0:T(8,128)(2,1)}, u32[]{:S(2)}) copy-start(bf16[64,2048]{1,0:T(8,128)(2,1)} %param.22) | copy-start | bytes 786436
  234.9 9.1 %copy-start.30 = (f32[1,2048]{1,0:T(1,128)S(1)}, f32[1,2048]{1,0:T(1,128)}, u32[]{:S(2)}) copy-start(f32[1,2048]{1,0:T(1,128)} %get-tuple-element.226) | copy-start | bytes 24580
  (11 other events, 22.2 us)
where the time goes:
time: 250 us; the launch traced here: 248 us
  blocking collectives  122 us (49%)
  local copies, waits for them, and re-layouts  58.6 us (23%)
  other arithmetic  34.5 us (14%)
  matrix products  28.4 us (11%)
  starting transfers between devices  3.15 us (1%)
    all_gather x4, blocking collectives, prefix(): lax.all_gather(a.astype(kind), axis)  54.2 us
    psum x1, blocking collectives, local(): lax.psum(jnp.dot(own_cols, modulation, preferred_element_type=jnp.float32...  39.4 us
    all_gather x1, blocking collectives, local(): context_cols = lax.all_gather(own_context, 'sp', axis=0, tiled=True)  14.5 us
    dot_general x10, matrix products, project_many(): jnp.dot(row_block, weight, preferred_element_type=jnp.float32)  10.5 us
    all_gather x1, blocking collectives, local(): lax.all_gather(hidden, 'tp', axis=0, tiled=True)  7.17 us
    all_to_all x1, blocking collectives, local(): lax.all_to_all(stacked, 'tp', split_axis=0, concat_axis=2, tiled=True)[0]  6.85 us
    another operation x3, other arithmetic  6.56 us
    exp x4, local copies, waits for them, and re-layouts, directed_pass(): jnp.exp(running)  5.96 us
  transfers between devices with their start and end apart: 2, of which 0 were waited for; matrix products, arithmetic and copies ran while one was open for 28% of the time, Pallas kernels for 0%

commit v1 on v0

--- a/solution.py
+++ b/solution.py
@@ -240,7 +240,12 @@
     own_context = project_many(
         modulated_norm(context, norm_gain, shift_rows[1], scale_rows[1]), context_mats
     )
-    context_cols = lax.all_gather(own_context, "sp", axis=0, tiled=True)
+    ring = [own_context]
+    for hop_ in range(3):
+        ring.append(lax.ppermute(ring[-1], "sp", [(dev, (dev + 1) % 4) for dev in range(4)]))
+    context_cols = jnp.roll(
+        jnp.concatenate(ring[::-1], axis=0), (lax.axis_index("sp") + 1) * ring[0].shape[0], axis=0
+    )
     ctx_span = head_cols + state_cols
     ctx_padded = jnp.pad(context_cols[:, :ctx_span], ((2, 1), (0, 0)))
     ctx_conv = conv_padded(

time: 250 us -> 257 us (1.028)
  waiting for transfers between devices: 0.01 us -> 11.1 us
  blocking collectives: 122 us -> 112 us
  local copies, waits for them, and re-layouts: 58.6 us -> 63.6 us
    all_gather x1 -> x0, blocking collectives: 14.5 us -> none  [local(): context_cols = lax.all_gather(own_context, 'sp', axis=0, tiled=True)]
    ppermute x0 -> x3, waiting for transfers between devices: none -> 11.1 us  [local(): lax.ppermute(ring[-1], 'sp', [(dev, (dev + 1) % 4) for dev in range(4)])]
    all_gather x4, blocking collectives: 54.2 us -> 59.1 us  [prefix(): lax.all_gather(a.astype(kind), axis)]
  transfers between devices with their start and end apart: 2 -> 5, of which waited for: 0 -> 2; matrix products, arithmetic and copies ran while one was open for 28% -> 32% of each run, Pallas kernels for 0% -> 0%
where the time goes in v1:
time: 257 us; the launch traced here: 254 us
  blocking collectives  112 us (44%)
  local copies, waits for them, and re-layouts  63.6 us (25%)
  other arithmetic  35.3 us (14%)
  matrix products  28.1 us (11%)
  waiting for transfers between devices  11.1 us (4%)
  starting transfers between devices  3.22 us (1%)
    all_gather x4, blocking collectives, prefix(): lax.all_gather(a.astype(kind), axis)  59.1 us
    psum x1, blocking collectives, local(): lax.psum(jnp.dot(own_cols, modulation, preferred_element_type=jnp.float32...  39.3 us
    ppermute x3, waiting for transfers between devices, local(): lax.ppermute(ring[-1], 'sp', [(dev, (dev + 1) % 4) for dev in range(4)])  11.1 us
    dot_general x10, matrix products, project_many(): jnp.dot(row_block, weight, preferred_element_type=jnp.float32)  8 us
    another operation x3, other arithmetic  7.18 us
    all_gather x1, blocking collectives, local(): lax.all_gather(hidden, 'tp', axis=0, tiled=True)  7.04 us
    all_to_all x1, blocking collectives, local(): lax.all_to_all(stacked, 'tp', split_axis=0, concat_axis=2, tiled=True)[0]  6.85 us
    exp x4, local copies, waits for them, and re-layouts, directed_pass(): jnp.exp(running)  5.93 us
  transfers between devices with their start and end apart: 5, of which 2 were waited for; matrix products, arithmetic and copies ran while one was open for 32% of the time, Pallas kernels for 0%

profile of v1, /device:TPU:0, one launch (start us, length us, event | category | flops | bytes accessed | tf_op | source)
XLA Modules:
  0.0 254.4 jit_solution(6130015616322045516)
XLA Ops:
  2.4 39.3 %psum.7 = f32[2,6144]{1,0:T(2,128)S(1)} all-reduce(f32[2,6144]{1,0:T(2,128)S(1)} %fusion.93), channel_id=1, replica_groups=mesh['sp'=4,'tp'=2,'dp'=4] {'sp','tp'}, use_global_device_ids=true, to_apply=%region_0.1 | all-reduce | flops 12288 | bytes 98304 | tf_op jit(solution)/shard_map/psum | solution.py:209
  43.7 1.6 convolution_convert_fusion.6
  48.2 7.0 %all_gather.23 = bf16[128,2048]{1,0:T(8,128)(2,1)S(1)} all-gather(bf16[64,2048]{1,0:T(8,128)(2,1)S(1)} %fusion.31), channel_id=1, replica_groups=mesh['sp'=4,'tp'=2,'dp'=4] {'tp'}, dimensions={0}, use_global_device_ids=true | all-gather | bytes 786432 | tf_op jit(solution)/shard_map/all_gather | solution.py:222
  57.4 1.9 collective-permute-start
  73.3 1.6 reduce_window_sum.52
  76.2 1.5 copy.188
  77.7 1.6 reduce_window_sum.56
  80.6 3.0 %divide_multiply_fusion = f32[128,512]{1,0:T(8,128)} fusion(bf16[128,2048]{1,0:T(8,128)(2,1)} %copy-done.1, bf16[2048,512]{1,0:T(8,128)(2,1)} %param.29), kind=kOutput, calls=%fused_computation.89 | convolution fusion | flops 268828672 | bytes 2883584 | tf_op jit(solution)/shard_map/dot_general | solution.py:63
  85.2 14.9 %all_gather.24 = bf16[4,2,4]{2,1,0:T(2,128)(2,1)} all-gather(bf16[1,2,4]{2,1,0:T(2,128)(2,1)S(1)} %copy-done.55), channel_id=1, replica_groups=mesh['sp'=4,'tp'=2,'dp'=4] {'sp'}, dimensions={0}, use_global_device_ids=true | all-gather | bytes 80 | tf_op jit(solution)/shard_map/all_gather | solution.py:19
  100.1 7.6 %all_gather.27 = bf16[4,2,4]{2,1,0:T(2,128)(2,1)} all-gather(bf16[1,2,4]{2,1,0:T(2,128)(2,1)S(1)} %copy-done.56), channel_id=1, replica_groups=mesh['sp'=4,'tp'=2,'dp'=4] {'sp'}, dimensions={0}, use_global_device_ids=true | all-gather | bytes 80 | tf_op jit(solution)/shard_map/all_gather | solution.py:19
  107.7 1.5 exp.128
  109.2 1.5 exp.139
  112.0 1.6 copy.176
  113.6 1.5 copy.174
  115.1 1.6 copy.189
  116.7 1.5 copy.187
  118.2 1.6 copy.185
  119.7 1.6 copy.172
  121.3 1.8 copy.190
  128.6 1.4 rev.19
  130.0 1.5 copy.167
  131.4 1.4 rev.20
  133.7 15.4 %all-gather = bf16[8,4,64,64]{3,2,1,0:T(8,128)(2,1)} all-gather(bf16[2,4,64,64]{3,2,1,0:T(8,128)(2,1)S(1)} %fusion.17), channel_id=2, replica_groups=mesh['sp'=4,'tp'=2,'dp'=4] {'sp'}, dimensions={0}, use_global_device_ids=true | all-gather | bytes 327680 | tf_op jit(solution)/shard_map/all_gather | solution.py:19
  151.0 1.7 copy.178
  152.7 1.5 copy.179
  156.0 21.2 %all-gather.1 = bf16[8,4,64,64]{3,2,1,0:T(8,128)(2,1)} all-gather(bf16[2,4,64,64]{3,2,1,0:T(8,128)(2,1)S(1)} %fusion.18), channel_id=3, replica_groups=mesh['sp'=4,'tp'=2,'dp'=4] {'sp'}, dimensions={0}, use_global_device_ids=true | all-gather | bytes 327680 | tf_op jit(solution)/shard_map/all_gather | solution.py:19
  178.5 9.1 %while.7 = (s32[]{:T(128)}, f32[2,4]{1,0:T(2,128)}, f32[2,4,64,64]{3,2,1,0:T(8,128)}, s32[]{:T(128)}, bf16[4,2,4]{2,1,0:T(2,128)(2,1)}, /*index=5*/bf16[4,2,4,64...) while((s32[]{:T(128)}, f32[2,4]{1,0:T(2,128)}, f32[2,4,64,64]{3,2,1,0:T(8,128)}, ...), condition=%wide.region_12.13_spmd, body=%wide.region_11.12_spmd.sunk | while | flops 98326 | bytes 327979 | solution.py:36
  179.8 1.8 convert_add_fusion.7
  182.8 1.8 convert_add_fusion.7
  185.8 1.8 convert_add_fusion.7
  188.9 1.5 copy.180
  190.3 1.6 convolution_bitcast_fusion.6
  192.0 1.7 copy.181
  193.6 1.6 convolution_bitcast_fusion.7
  195.3 1.6 copy.168
  197.0 1.7 fusion.11
  198.7 5.6 %collective-permute-done.3 = bf16[128,656]{0,1:T(8,128)(2,1)S(1)} collective-permute-done((bf16[128,656]{0,1:T(8,128)(2,1)}, bf16[128,656]{0,1:T(8,128)(2,1)S(1)}, u32[]{:S(2)}, u32[]{:S(2)}) %collective-permute-start.3) | collective-permute-done | bytes 167968 | tf_op jit(solution)/shard_map/ppermute | solution.py:245
  204.4 1.7 fusion.13
  206.1 5.4 %collective-permute-done.4 = bf16[128,656]{0,1:T(8,128)(2,1)S(1)} collective-permute-done((bf16[128,656]{0,1:T(8,128)(2,1)S(1)}, bf16[128,656]{0,1:T(8,128)(2,1)S(1)}, u32[]{:S(2)}, u32[]{:S(2)}) %collective-permute-start.4) | collective-permute-done | bytes 167968 | tf_op jit(solution)/shard_map/ppermute | solution.py:245
  216.2 1.6 multiply_convert_fusion
  218.7 5.1 %reduce-window.6 = f32[2,8,4,128]{3,1,2,0:T(8,128)} reduce-window(f32[2,8,4,128]{3,1,2,0:T(8,128)} %fusion.148, f32[]{:T(128)} %constant.148.clone.1), window={size=1x1x1x128 pad=0_0x0_0x0_0x127_0}, to_apply=%region_7.8 | reduce-window | flops 1040384 | bytes 65540 | tf_op jit(solution)/shard_map/reduce-window
  223.8 1.5 slice_reduce_fusion
  228.3 1.4 fusion.76
  232.4 1.8 fusion.15
  236.4 1.8 rev.23
  238.2 1.8 fusion.16
  243.6 6.8 %all_to_all.15 = bf16[2,64,512]{2,1,0:T(8,128)(2,1)S(1)} all-to-all(bf16[2,64,512]{2,1,0:T(8,128)(2,1)S(1)} %copy.199), channel_id=1, replica_groups=mesh['sp'=4,'tp'=2,'dp'=4] {'tp'}, dimensions={0} | all-to-all | bytes 262144 | tf_op jit(solution)/shard_map/all_to_all | solution.py:286
  250.7 3.8 %fusion.1 = bf16[64,2048]{1,0:T(8,128)(2,1)} fusion(bf16[64,1024]{1,0:T(8,128)(2,1)S(1)} %bitcast.213, bf16[1024,2048]{1,0:T(8,128)(2,1)} %param.39, bf16[64,2048]{1,0:T(8,128)(2,1)S(1)} %copy-done.3, f32[2048]{0:T(1024)S(1)} %bitcast.239), kind=kOutput, calls=%fused_computation.10 | convolution fusion | flops 268959744 | bytes 4857856 | tf_op jit(solution)/shard_map/dot_general | solution.py:285
  (227 shorter events, 62.1 us)
Async XLA Ops:
  1.9 40.5 %copy-start.49 = (bf16[2048]{0:T(1024)(128)(2,1)S(1)}, bf16[2048]{0:T(1024)(128)(2,1)}, u32[]{:S(2)}) copy-start(bf16[2048]{0:T(1024)(128)(2,1)} %param.27) | copy-start | bytes 12292
  1.9 41.7 %copy-start.30 = (bf16[2,2048,8]{1,2,0:T(8,128)(2,1)S(1)}, bf16[2,2048,8]{1,2,0:T(8,128)(2,1)}, u32[]{:S(2)}) copy-start(bf16[2,2048,8]{1,2,0:T(8,128)(2,1)} %param.32) | copy-start | bytes 196612
  41.8 3.5 %copy-start.14 = (bf16[128,2048]{1,0:T(8,128)(2,1)S(1)}, bf16[128,2048]{1,0:T(8,128)(2,1)}, u32[]{:S(2)}) copy-start(bf16[128,2048]{1,0:T(8,128)(2,1)} %param.24) | copy-start | bytes 1572868
  43.6 2.0 copy-start.4
  47.9 149.1 %collective-permute-start.2 = (bf16[128,656]{0,1:T(8,128)(2,1)}, bf16[128,656]{0,1:T(8,128)(2,1)}, u32[]{:S(2)}, u32[]{:S(2)}) collective-permute-start(bf16[128,656]{0,1:T(8,128)(2,1)} %pad_maximum_fusion), channel_id=1, source_target_pairs={{0,8},{8,16},{16,24},{24,0},{1,9},{9,17},{17,25},{25,1},{2,10},{10... | collective-permute-start | bytes 503816 | tf_op jit(solution)/shard_map/ppermute | solution.py:245
  55.2 5.6 %copy-start.1 = (bf16[128,2048]{1,0:T(8,128)(2,1)}, bf16[128,2048]{1,0:T(8,128)(2,1)S(1)}, u32[]{:S(2)}) copy-start(bf16[128,2048]{1,0:T(8,128)(2,1)S(1)} %all_gather.23) | copy-start | bytes 1572868
  55.7 5.1 %copy-start.7 = (bf16[128,512]{1,0:T(8,128)(2,1)}, bf16[128,512]{1,0:T(8,128)(2,1)S(1)}, u32[]{:S(2)}) copy-start(bf16[128,512]{1,0:T(8,128)(2,1)S(1)} %convolution_convert_fusion.2) | copy-start | bytes 393220
  56.5 5.4 %copy-start.21 = (bf16[128,128]{1,0:T(8,128)(2,1)}, bf16[128,128]{1,0:T(8,128)(2,1)S(1)}, u32[]{:S(2)}) copy-start(bf16[128,128]{1,0:T(8,128)(2,1)S(1)} %convolution_convert_fusion.5) | copy-start | bytes 98308
  56.5 4.6 %copy-start.54 = (f32[2,8]{1,0:T(2,128)S(1)}, f32[2,8]{1,0:T(2,128)}, u32[]{:S(2)}) copy-start(f32[2,8]{1,0:T(2,128)} %param.36) | copy-start | bytes 196
  56.5 4.7 %copy-start.53 = (f32[128,8]{0,1:T(8,128)S(1)}, f32[128,8]{0,1:T(8,128)}, u32[]{:S(2)}) copy-start(f32[128,8]{0,1:T(8,128)} %param.37) | copy-start | bytes 12292
  56.8 5.1 %copy-start.22 = (bf16[128,128]{1,0:T(8,128)(2,1)}, bf16[128,128]{1,0:T(8,128)(2,1)S(1)}, u32[]{:S(2)}) copy-start(bf16[128,128]{1,0:T(8,128)(2,1)S(1)} %convolution_convert_fusion.4) | copy-start | bytes 98308
  57.4 67.1 %collective-permute-start = (bf16[2,768]{1,0:T(2,128)(2,1)}, bf16[2,768]{1,0:T(2,128)(2,1)}, u32[]{:S(2)}, u32[]{:S(2)}) collective-permute-start(bf16[2,768]{1,0:T(2,128)(2,1)} %get-tuple-element.220), channel_id=1, source_target_pairs={{0,8},{8,16},{16,24},{1,9},{9,17},{17,25},{2,10},{10,18},{18,26},{... | collective-permute-start | bytes 9224 | tf_op jit(solution)/shard_map/ppermute | solution.py:44
  59.3 65.2 %collective-permute-start.1 = (bf16[2,768]{1,0:T(2,128)(2,1)}, bf16[2,768]{1,0:T(2,128)(2,1)}, u32[]{:S(2)}, u32[]{:S(2)}) collective-permute-start(bf16[2,768]{1,0:T(2,128)(2,1)} %get-tuple-element.221), channel_id=1, source_target_pairs={{8,0},{16,8},{24,16},{9,1},{17,9},{25,17},{10,2},{18,10},{26,18},{... | collective-permute-start | bytes 9224 | tf_op jit(solution)/shard_map/ppermute | solution.py:47
  60.9 22.8 %copy-start.28 = (f32[128,8]{0,1:T(8,128)}, f32[128,8]{0,1:T(8,128)S(1)}, u32[]{:S(2)}) copy-start(f32[128,8]{0,1:T(8,128)S(1)} %compare_select_fusion.3) | copy-start | bytes 12292
  80.6 3.0 %copy-start.51 = (f32[2,4]{1,0:T(2,128)S(1)}, f32[2,4]{1,0:T(2,128)}, u32[]{:S(2)}) copy-start(f32[2,4]{1,0:T(2,128)} %slice_bitcast_fusion.3) | copy-start | bytes 100
  80.6 3.0 %copy-start.18 = (f32[128,2,4]{2,1,0:T(2,128)S(1)}, f32[128,2,4]{2,1,0:T(2,128)}, u32[]{:S(2)}) copy-start(f32[128,2,4]{2,1,0:T(2,128)} %copy.175) | copy-start | bytes 12292
  80.6 3.8 %copy-start.52 = (f32[2,4]{1,0:T(2,128)S(1)}, f32[2,4]{1,0:T(2,128)}, u32[]{:S(2)}) copy-start(f32[2,4]{1,0:T(2,128)} %slice_bitcast_fusion.2) | copy-start | bytes 100
  80.6 3.8 %copy-start.19 = (f32[128,2,4]{2,1,0:T(2,128)S(1)}, f32[128,2,4]{2,1,0:T(2,128)}, u32[]{:S(2)}) copy-start(f32[128,2,4]{2,1,0:T(2,128)} %copy.188) | copy-start | bytes 12292
  80.6 4.6 %copy-start.55 = (bf16[1,2,4]{2,1,0:T(2,128)(2,1)S(1)}, bf16[1,2,4]{2,1,0:T(2,128)(2,1)}, u32[]{:S(2)}) copy-start(bf16[1,2,4]{2,1,0:T(2,128)(2,1)} %convert_element_type.233) | copy-start | bytes 52
  80.6 19.5 %copy-start.56 = (bf16[1,2,4]{2,1,0:T(2,128)(2,1)S(1)}, bf16[1,2,4]{2,1,0:T(2,128)(2,1)}, u32[]{:S(2)}) copy-start(bf16[1,2,4]{2,1,0:T(2,128)(2,1)} %convert_element_type.248) | copy-start | bytes 52
  111.3 13.2 %copy-start.8 = (bf16[128,512]{1,0:T(8,128)(2,1)S(1)}, bf16[128,512]{1,0:T(8,128)(2,1)}, u32[]{:S(2)}) copy-start(bf16[128,512]{1,0:T(8,128)(2,1)} %copy-done.7) | copy-start | bytes 393220
  112.0 13.3 %copy-start.37 = (f32[768]{0:T(1024)S(1)}, f32[768]{0:T(1024)}, u32[]{:S(2)}) copy-start(f32[768]{0:T(1024)} %get-tuple-element.178) | copy-start | bytes 9220
  112.0 13.3 %copy-start.38 = (f32[768]{0:T(1024)S(1)}, f32[768]{0:T(1024)}, u32[]{:S(2)}) copy-start(f32[768]{0:T(1024)} %get-tuple-element.179) | copy-start | bytes 9220
  112.0 13.3 %copy-start.39 = (f32[768]{0:T(1024)S(1)}, f32[768]{0:T(1024)}, u32[]{:S(2)}) copy-start(f32[768]{0:T(1024)} %get-tuple-element.180) | copy-start | bytes 9220
  112.0 13.3 %copy-start.40 = (f32[768]{0:T(1024)S(1)}, f32[768]{0:T(1024)}, u32[]{:S(2)}) copy-start(f32[768]{0:T(1024)} %get-tuple-element.181) | copy-start | bytes 9220
  126.4 22.8 %copy-start.5 = (bf16[128,512]{0,1:T(8,128)(2,1)}, bf16[128,512]{0,1:T(8,128)(2,1)S(1)}, u32[]{:S(2)}) copy-start(bf16[128,512]{0,1:T(8,128)(2,1)S(1)} %copy.165) | copy-start | bytes 393220
  128.6 20.6 %copy-start.23 = (bf16[128,128]{0,1:T(8,128)(2,1)}, bf16[128,128]{0,1:T(8,128)(2,1)S(1)}, u32[]{:S(2)}) copy-start(bf16[128,128]{0,1:T(8,128)(2,1)S(1)} %copy.166) | copy-start | bytes 98308
  196.9 15.7 %copy-start.25 = (bf16[128,128]{0,1:T(8,128)(2,1)S(1)}, bf16[128,128]{0,1:T(8,128)(2,1)}, u32[]{:S(2)}) copy-start(bf16[128,128]{0,1:T(8,128)(2,1)} %copy-done.24) | copy-start | bytes 98308
  196.9 15.7 %copy-start.34 = (bf16[128,8]{0,1:T(8,128)(2,1)S(1)}, bf16[128,8]{0,1:T(8,128)(2,1)}, u32[]{:S(2)}) copy-start(bf16[128,8]{0,1:T(8,128)(2,1)} %copy-done.33) | copy-start | bytes 6148
  196.9 15.7 %copy-start.36 = (bf16[128,8]{0,1:T(8,128)(2,1)S(1)}, bf16[128,8]{0,1:T(8,128)(2,1)}, u32[]{:S(2)}) copy-start(bf16[128,8]{0,1:T(8,128)(2,1)} %copy-done.35) | copy-start | bytes 6148
  196.9 7.4 %collective-permute-start.3 = (bf16[128,656]{0,1:T(8,128)(2,1)}, bf16[128,656]{0,1:T(8,128)(2,1)S(1)}, u32[]{:S(2)}, u32[]{:S(2)}) collective-permute-start(bf16[128,656]{0,1:T(8,128)(2,1)} %collective-permute-done.2), channel_id=1, source_target_pairs={{0,8},{8,16},{16,24},{24,0},{1,9},{9,17},{17,25},{25,1},{2,10},{10... | collective-permute-start | bytes 503816 | tf_op jit(solution)/shard_map/ppermute | solution.py:245
  204.4 7.2 %collective-permute-start.4 = (bf16[128,656]{0,1:T(8,128)(2,1)S(1)}, bf16[128,656]{0,1:T(8,128)(2,1)S(1)}, u32[]{:S(2)}, u32[]{:S(2)}) collective-permute-start(bf16[128,656]{0,1:T(8,128)(2,1)S(1)} %collective-permute-done.3), channel_id=1, source_target_pairs={{0,8},{8,16},{16,24},{24,0},{1,9},{9,17},{17,25},{25,1},{2,10},{10... | collective-permute-start | bytes 503816 | tf_op jit(solution)/shard_map/ppermute | solution.py:245
  206.1 7.8 %copy-start.43 = (f32[2,8]{1,0:T(2,128)S(1)}, f32[2,8]{1,0:T(2,128)}, u32[]{:S(2)}) copy-start(f32[2,8]{1,0:T(2,128)} %copy-done.42) | copy-start | bytes 196
  218.7 16.5 %copy-start.9 = (bf16[512,128]{0,1:T(8,128)(2,1)}, bf16[512,128]{0,1:T(8,128)(2,1)S(1)}, u32[]{:S(2)}) copy-start(bf16[512,128]{0,1:T(8,128)(2,1)S(1)} %slice.228) | copy-start | bytes 393220
  232.4 2.9 %copy-start.17 = (bf16[128,512]{0,1:T(8,128)(2,1)S(1)}, bf16[128,512]{0,1:T(8,128)(2,1)}, u32[]{:S(2)}) copy-start(bf16[128,512]{0,1:T(8,128)(2,1)} %copy.178) | copy-start | bytes 393220
  232.4 2.9 %copy-start.26 = (f32[128,2,4,64]{0,3,2,1:T(8,128)S(1)}, f32[128,2,4,64]{0,3,2,1:T(8,128)}, u32[]{:S(2)}) copy-start(f32[128,2,4,64]{0,3,2,1:T(8,128)} %fusion.11) | copy-start | bytes 786436
  232.4 2.9 %copy-start.27 = (f32[128,128,2]{1,0,2:T(8,128)S(1)}, f32[128,128,2]{1,0,2:T(8,128)}, u32[]{:S(2)}) copy-start(f32[128,128,2]{1,0,2:T(8,128)} %copy.181) | copy-start | bytes 393220
  232.4 2.9 %copy-start.44 = (f32[128,8]{0,1:T(8,128)S(1)}, f32[128,8]{0,1:T(8,128)}, u32[]{:S(2)}) copy-start(f32[128,8]{0,1:T(8,128)} %rev.22) | copy-start | bytes 12292
  232.4 2.9 %copy-start.50 = (f32[128,2,4]{0,2,1:T(4,128)S(1)}, f32[128,2,4]{0,2,1:T(4,128)}, u32[]{:S(2)}) copy-start(f32[128,2,4]{0,2,1:T(4,128)} %copy.183) | copy-start | bytes 12292
  236.4 4.7 %copy-start.6 = (bf16[128,512]{0,1:T(8,128)(2,1)S(1)}, bf16[128,512]{0,1:T(8,128)(2,1)}, u32[]{:S(2)}) copy-start(bf16[128,512]{0,1:T(8,128)(2,1)} %copy-done.5) | copy-start | bytes 393220
  238.2 2.9 %copy-start.10 = (f32[128,512]{0,1:T(8,128)S(1)}, f32[128,512]{0,1:T(8,128)}, u32[]{:S(2)}) copy-start(f32[128,512]{0,1:T(8,128)} %copy.190) | copy-start | bytes 786436
  238.2 2.9 %copy-start.11 = (f32[128,2,4,64]{0,3,2,1:T(8,128)S(1)}, f32[128,2,4,64]{0,3,2,1:T(8,128)}, u32[]{:S(2)}) copy-start(f32[128,2,4,64]{0,3,2,1:T(8,128)} %fusion.13) | copy-start | bytes 786436
  238.2 2.9 %copy-start.12 = (f32[128,2,4,64]{0,3,2,1:T(8,128)S(1)}, f32[128,2,4,64]{0,3,2,1:T(8,128)}, u32[]{:S(2)}) copy-start(f32[128,2,4,64]{0,3,2,1:T(8,128)} %rev.23) | copy-start | bytes 786436
  238.2 2.9 %copy-start.20 = (f32[128,128,2]{1,0,2:T(8,128)S(1)}, f32[128,128,2]{1,0,2:T(8,128)}, u32[]{:S(2)}) copy-start(f32[128,128,2]{1,0,2:T(8,128)} %copy.168) | copy-start | bytes 393220
  238.2 2.9 %copy-start.29 = (f32[128,8]{0,1:T(8,128)S(1)}, f32[128,8]{0,1:T(8,128)}, u32[]{:S(2)}) copy-start(f32[128,8]{0,1:T(8,128)} %copy-done.28) | copy-start | bytes 12292
  238.2 2.9 %copy-start.31 = (f32[128,2,4]{0,2,1:T(4,128)S(1)}, f32[128,2,4]{0,2,1:T(4,128)}, u32[]{:S(2)}) copy-start(f32[128,2,4]{0,2,1:T(4,128)} %copy.170) | copy-start | bytes 12292
  241.5 9.1 %copy-start.3 = (bf16[64,2048]{1,0:T(8,128)(2,1)S(1)}, bf16[64,2048]{1,0:T(8,128)(2,1)}, u32[]{:S(2)}) copy-start(bf16[64,2048]{1,0:T(8,128)(2,1)} %param.22) | copy-start | bytes 786436
  241.5 9.1 %copy-start.32 = (f32[1,2048]{1,0:T(1,128)S(1)}, f32[1,2048]{1,0:T(1,128)}, u32[]{:S(2)}) copy-start(f32[1,2048]{1,0:T(1,128)} %get-tuple-element.226) | copy-start | bytes 24580
  (14 other events, 16.3 us)
